TPU v7x, 32 devices: a whole 2x2x4 slice. The times are simulated.
32 devices in a mesh: rep: 2 (over x), fs: 4 (over z), tp: 4 (over y, core).
Axes of the slice: x: 2, y: 2, z: 4, core: 2. Of those that a mesh axis runs over, the one named last changes fastest.
Arguments:
- tokens: bfloat16 [4096, 2048], P(('rep', 'fs', 'tp')), may hold values from -6 to 6
- mixer_gain: float32 [2048], replicated, may hold values from 0.1 to 1.9
- direct_weight: float32 [2048, 1024], P('fs', 'tp'), may hold values from -0.125 to 0.125
- direct_scale: float32 [1024], P('tp'), may hold values from 0.5 to 2
- value_weight: float32 [2048, 1024], P('fs', 'tp'), may hold values from -0.125 to 0.125
- value_scale: float32 [1024], P('tp'), may hold values from 0.5 to 8, as said below
- value_gain: float32 [1024], P('tp'), may hold values from 0.1 to 1.9
- value_shift: float32 [1024], P('tp'), may hold values from -3 to 3
- spatial_weight: bfloat16 [16, 128, 128], P('tp'), may hold values from -0.25 to 0.25
- spatial_bias: float32 [16, 128], P('tp'), may hold values from 0.1 to 1.9
- merge_weight: float32 [1024, 2048], P('tp', 'fs'), may hold values from -0.1875 to 0.1875
- merge_scale: float32 [2048], P('fs'), may hold values from 0.5 to 2
- channel_gain: float32 [2048], replicated, may hold values from 0.1 to 1.9
- expand_weight: float32 [2048, 8192], P('fs', 'tp'), may hold values from -0.125 to 0.125
- expand_scale: float32 [8192], P('tp'), may hold values from 0.5 to 2
- reduce_weight: float32 [8192, 2048], P('tp', 'fs'), may hold values from -0.0625 to 0.0625
- reduce_scale: float32 [2048], P('fs'), may hold values from 0.5 to 2
Outputs:
- result: bfloat16 [4096, 2048], P(('rep', 'fs', 'tp'))
Inputs may be any that keep to these rules, and one draw needn't show every extreme that they name: `value_scale`: positive column scales.
All inputs are finite; a program needn't handle non-finite values.
Results may differ from a plain program's by a relative error of at most 0.024.
Values may be sent and summed in bfloat16 or wider, within the bound.
A program may use at most 64 MiB of HBM per device.

v0:
```python
import jax
import jax.numpy as jnp
from jax import lax
from jax.sharding import PartitionSpec as P

GDIM = 64
BLOCK = 128
epsilon = 1e-06


def rms_rows(rows, gain):
    floats = rows.astype(jnp.float32)
    scaled = floats * lax.rsqrt(jnp.mean(floats * floats, axis=-1, keepdims=True) + epsilon)
    return (scaled * gain).astype(jnp.bfloat16)


def body(
    tokens,
    mixer_gain,
    direct_weight,
    direct_scale,
    value_weight,
    value_scale,
    value_gain,
    value_shift,
    spatial_weight,
    spatial_bias,
    merge_weight,
    merge_scale,
    channel_gain,
    expand_weight,
    expand_scale,
    reduce_weight,
    reduce_scale,
):
    direct_half = direct_weight.astype(jnp.bfloat16)
    value_half = value_weight.astype(jnp.bfloat16)
    merge_half = merge_weight.astype(jnp.bfloat16)
    expand_half = expand_weight.astype(jnp.bfloat16)
    reduce_half = reduce_weight.astype(jnp.bfloat16)
    full_expand, full_reduce, reduce_full_scale = (
        lax.all_gather(expand_half, "fs", axis=0, tiled=True),
        lax.all_gather(reduce_half, "fs", axis=1, tiled=True),
        lax.all_gather(reduce_scale.astype(jnp.bfloat16), "fs", axis=0, tiled=True).astype(
            reduce_scale.dtype
        ),
    )
    normed = rms_rows(tokens, mixer_gain)
    whole = lax.all_gather(normed, "tp", axis=0, tiled=True)
    seq_rows = whole.shape[0]
    local_width = direct_weight.shape[1]
    direct_pre = jnp.dot(
        whole,
        lax.all_gather(direct_half, "fs", axis=0, tiled=True),
        preferred_element_type=jnp.float32,
    )
    value_pre = jnp.dot(
        whole,
        lax.all_gather(value_half, "fs", axis=0, tiled=True),
        preferred_element_type=jnp.float32,
    )
    full_merge, merge_full_scale = (
        lax.all_gather(merge_half, "fs", axis=1, tiled=True),
        lax.all_gather(merge_scale.astype(jnp.bfloat16), "fs", axis=0, tiled=True).astype(
            merge_scale.dtype
        ),
    )
    direct = jax.nn.gelu(direct_pre * direct_scale)
    value = jax.nn.gelu(value_pre * value_scale)
    total, squares = lax.psum((jnp.sum(value, axis=1), jnp.sum(value * value, axis=1)), "tp")
    branch_width = local_width * lax.axis_size("tp")
    mean = (total / branch_width)[:, None]
    var = (squares / branch_width)[:, None] - mean * mean
    gated_value = ((value - mean) * lax.rsqrt(var + epsilon) * value_gain + value_shift).astype(
        jnp.bfloat16
    )
    local_groups = spatial_weight.shape[0]
    blocks = gated_value.reshape(seq_rows // BLOCK, BLOCK, local_groups, GDIM)
    mixed = jnp.einsum("gpq,nqgc->npgc", spatial_weight, blocks, preferred_element_type=jnp.float32)
    mixed = mixed + jnp.transpose(spatial_bias)[None, :, :, None]
    gated = (direct * mixed.reshape(seq_rows, local_width)).astype(jnp.bfloat16)
    rows = gated
    mix = lax.psum_scatter(
        (jnp.dot(rows, full_merge, preferred_element_type=jnp.float32) * merge_full_scale).astype(
            jnp.bfloat16
        ),
        "tp",
        scatter_dimension=0,
        tiled=True,
    ).astype(jnp.float32)
    middle = (tokens.astype(jnp.float32) + mix).astype(jnp.bfloat16)
    normed_mid = rms_rows(middle, channel_gain)
    whole_mid = lax.all_gather(normed_mid, "tp", axis=0, tiled=True)
    upper = jnp.dot(whole_mid, full_expand, preferred_element_type=jnp.float32)
    hidden = jnp.square(jax.nn.relu(upper * expand_scale)).astype(jnp.bfloat16)
    rows = hidden
    lower = lax.psum_scatter(
        (jnp.dot(rows, full_reduce, preferred_element_type=jnp.float32) * reduce_full_scale).astype(
            jnp.bfloat16
        ),
        "tp",
        scatter_dimension=0,
        tiled=True,
    ).astype(jnp.float32)
    return (middle.astype(jnp.float32) + lower).astype(jnp.bfloat16)


def solution(mesh):
    return jax.shard_map(
        body,
        mesh=mesh,
        in_specs=(
            P(("rep", "fs", "tp"), None),
            P(),
            P("fs", "tp"),
            P("tp"),
            P("fs", "tp"),
            P("tp"),
            P("tp"),
            P("tp"),
            P("tp", None, None),
            P("tp", None),
            P("tp", "fs"),
            P("fs"),
            P(),
            P("fs", "tp"),
            P("tp"),
            P("tp", "fs"),
            P("fs"),
        ),
        out_specs=P(("rep", "fs", "tp"), None),
        check_vma=False,
    )
```

profile of v0, /device:TPU:0, one launch (start us, length us, event | category | flops | bytes accessed | tf_op | source)
XLA Modules:
  0.0 539.8 jit_solution(16502499518747901413)
XLA Ops:
  6.5 0.0 all-gather.14.cloned.1.call-start
  6.6 1.8 convert_element_type.71
  8.4 0.0 all-gather.14.cloned.1.call-update
  8.4 0.0 all-gather.10.cloned.1.call-start
  8.5 1.2 fusion.1
  9.7 2.0 fusion.3
  11.7 0.0 all-gather.10.cloned.1.call-update
  11.8 0.0 all-gather.12.cloned.1.call-start
  11.8 1.8 convert_element_type.70
  13.6 0.0 all-gather.12.cloned.1.call-update
  13.6 0.0 all-gather.16.cloned.1.call-start
  13.7 0.7 convert_element_type.74
  14.4 0.0 all-gather.16.cloned.1.call-update
  14.4 0.0 reduce-scatter.3.cloned.1.call-start
  14.5 13.9 %all-gather = bf16[4,1,512]{2,1,0:T(2,128)(2,1)S(1)} all-gather(bf16[1,1,512]{2,1,0:T(2,128)(2,1)S(1)} %reshape.40), channel_id=1, replica_groups=mesh['rep'=2,'fs'=4,'tp'=4] {'fs'}, dimensions={0}, use_global_device_ids=true | all-gather | bytes 5120 | tf_op jit(solution)/shard_map/all_gather | solution.py:64
  28.4 11.3 %all-gather.14.cloned.1.call-done = bf16[2048,256]{1,0:T(8,128)(2,1)} async-done(((bf16[512,256]{1,0:T(8,128)(2,1)}), bf16[2048,256]{1,0:T(8,128)(2,1)}) %all-gather.14.cloned.1.call-update) | async-done | bytes 1048592 | tf_op jit(solution)/shard_map/all_gather | solution.py:59
  39.7 23.5 %all-gather.10.cloned.1.call-done = bf16[512,2048]{1,0:T(8,128)(2,1)} async-done(((bf16[128,2048]{1,0:T(8,128)(2,1)}), bf16[512,2048]{1,0:T(8,128)(2,1)}) %all-gather.10.cloned.1.call-update) | async-done | bytes 2097168 | tf_op jit(solution)/shard_map/all_gather | solution.py:49
  63.3 2.8 fusion.37
  66.1 5.9 %all-reduce = (f32[512]{0:T(512)S(1)}, f32[512]{0:T(512)S(1)}) all-reduce(f32[512]{0:T(512)S(1)} %get-tuple-element.6, f32[512]{0:T(512)S(1)} %get-tuple-element.5), channel_id=1, replica_groups=mesh['rep'=2,'fs'=4,'tp'=4] {'tp'}, use_global_device_ids=true, to_apply=%region_4.0 | all-reduce | flops 1024 | bytes 8192 | tf_op jit(solution)/shard_map/psum | solution.py:70
  72.0 0.2 add_convert_fusion
  72.2 0.2 reshape.47
  72.5 0.3 fusion
  72.8 0.4 copy.35
  73.2 0.6 reshape.48
  73.8 19.1 %all-gather.12.cloned.1.call-done = bf16[2048,256]{1,0:T(8,128)(2,1)} async-done(((bf16[512,256]{1,0:T(8,128)(2,1)}), bf16[2048,256]{1,0:T(8,128)(2,1)}) %all-gather.12.cloned.1.call-update) | async-done | bytes 1048592 | tf_op jit(solution)/shard_map/all_gather | solution.py:54
  92.9 28.8 %all-gather.16.cloned.1.call-done = bf16[256,2048]{1,0:T(8,128)(2,1)} async-done(((bf16[256,512]{1,0:T(8,128)(2,1)}), bf16[256,2048]{1,0:T(8,128)(2,1)}) %all-gather.16.cloned.1.call-update) | async-done | bytes 1048592 | tf_op jit(solution)/shard_map/all_gather | solution.py:63
  121.7 5.9 %multiply_convert_fusion.2 = bf16[512,2048]{1,0:T(8,128)(2,1)} fusion(bf16[256,2048]{1,0:T(8,128)(2,1)} %all-gather.16.cloned.1.call-done, f32[2048]{0:T(1024)S(1)} %bitcast.20, f32[512,256]{1,0:T(8,128)S(1)} %reshape.48, bf16[512,2048]{1,0:T(8,128)(2,1)} %all-gather.10.cloned.1.call-done, bf16[2048,256]{1,0:T(8,128)(2,1)} %all-gather.12.cloned.1.call-done, ...), kind=kOutput, calls=%fused_computation.2 | convolution fusion | flops 1077280768 | bytes 6824960 | tf_op jit(solution)/shard_map/dot_general | solution.py:84
  127.6 0.0 reduce-scatter.3.cloned.1.call-update
  127.6 0.0 all-gather.18.cloned.1.call-start
  127.7 30.7 %reduce-scatter.3.cloned.1.call-done = bf16[128,2048]{1,0:T(8,128)(2,1)} async-done(((bf16[512,2048]{1,0:T(8,128)(2,1)}), bf16[128,2048]{1,0:T(8,128)(2,1)}) %reduce-scatter.3.cloned.1.call-update) | async-done | bytes 524304 | tf_op jit(solution)/shard_map/reduce_scatter | solution.py:83
  158.3 1.3 fusion.5
  159.7 2.0 fusion.7
  161.7 0.0 all-gather.18.cloned.1.call-update
  161.7 0.0 all-gather.20.cloned.1.call-start
  161.8 3.8 convert_element_type.82
  165.6 0.0 all-gather.20.cloned.1.call-update
  165.6 0.0 all-gather.22.cloned.1.call-start
  165.7 3.9 convert_element_type.84
  169.5 0.0 all-gather.22.cloned.1.call-update
  169.6 0.0 reduce-scatter.5.cloned.1.call-start
  169.6 12.1 %all-gather.1 = bf16[4,1,512]{2,1,0:T(2,128)(2,1)S(1)} all-gather(bf16[1,1,512]{2,1,0:T(2,128)(2,1)S(1)} %reshape.42), channel_id=1, replica_groups=mesh['rep'=2,'fs'=4,'tp'=4] {'fs'}, dimensions={0}, use_global_device_ids=true | all-gather | bytes 5120 | tf_op jit(solution)/shard_map/all_gather | solution.py:44
  181.8 2.7 all-gather.18.cloned.1.call-done
  184.4 151.2 %all-gather.20.cloned.1.call-done = bf16[2048,2048]{1,0:T(8,128)(2,1)} async-done(((bf16[512,2048]{1,0:T(8,128)(2,1)}), bf16[2048,2048]{1,0:T(8,128)(2,1)}) %all-gather.20.cloned.1.call-update) | async-done | bytes 8388624 | tf_op jit(solution)/shard_map/all_gather | solution.py:42
  335.7 149.4 %all-gather.22.cloned.1.call-done = bf16[2048,2048]{1,0:T(8,128)(2,1)} async-done(((bf16[2048,512]{1,0:T(8,128)(2,1)}), bf16[2048,2048]{1,0:T(8,128)(2,1)}) %all-gather.22.cloned.1.call-update) | async-done | bytes 8388624 | tf_op jit(solution)/shard_map/all_gather | solution.py:43
  485.1 16.6 %multiply_convert_fusion = bf16[512,2048]{1,0:T(8,128)(2,1)} fusion(bf16[2048,2048]{1,0:T(8,128)(2,1)} %all-gather.22.cloned.1.call-done, f32[2048]{0:T(1024)S(1)} %bitcast.21, bf16[512,2048]{1,0:T(8,128)(2,1)} %all-gather.18.cloned.1.call-done, bf16[2048,2048]{1,0:T(8,128)(2,1)} %all-gather.20.cloned.1.call-done, f32[2048]{0:T(1024)S(1)} %copy-done.10), kind=kOutput, calls=%fused_computation | convolution fusion | flops 8596226048 | bytes 20987904 | tf_op jit(solution)/shard_map/dot_general | solution.py:98
  501.6 0.0 reduce-scatter.5.cloned.1.call-update
  501.6 29.5 %reduce-scatter.5.cloned.1.call-done = bf16[128,2048]{1,0:T(8,128)(2,1)} async-done(((bf16[512,2048]{1,0:T(8,128)(2,1)}), bf16[128,2048]{1,0:T(8,128)(2,1)}) %reduce-scatter.5.cloned.1.call-update) | async-done | bytes 524304 | tf_op jit(solution)/shard_map/reduce_scatter | solution.py:97
  531.2 2.1 fusion.8
  (35 shorter events, 0.1 us)
Async XLA Ops:
  6.5 65.9 %copy-start = (bf16[4,128,128]{2,1,0:T(8,128)(2,1)S(1)}, bf16[4,128,128]{2,1,0:T(8,128)(2,1)}, u32[]{:S(2)}) copy-start(bf16[4,128,128]{2,1,0:T(8,128)(2,1)} %param.25) | copy-start | bytes 393220
  6.5 7.1 %copy-start.3 = (f32[256,512]{1,0:T(8,128)S(1)}, f32[256,512]{1,0:T(8,128)}, u32[]{:S(2)}) copy-start(f32[256,512]{1,0:T(8,128)} %param.27) | copy-start | bytes 1572868
  6.5 7.9 %copy-start.6 = (f32[512]{0:T(512)S(1)}, f32[512]{0:T(512)}, u32[]{:S(2)}) copy-start(f32[512]{0:T(512)} %param.28) | copy-start | bytes 6148
  6.5 56.7 %copy-start.11 = (f32[256]{0:T(256)S(1)}, f32[256]{0:T(256)}, u32[]{:S(2)}) copy-start(f32[256]{0:T(256)} %param.22) | copy-start | bytes 3076
  6.5 33.2 %all-gather.14.cloned.1.call-start = ((), (), s32[]{:S(2)}) async-start(), calls=%async_computation.4 | async-start | bytes 1310720 | tf_op jit(solution)/shard_map/all_gather | solution.py:59
  8.4 54.8 %all-gather.10.cloned.1.call-start = ((), (), s32[]{:S(2)}) async-start(), calls=%async_computation.2 | async-start | bytes 2621440 | tf_op jit(solution)/shard_map/all_gather | solution.py:49
  11.8 81.1 %all-gather.12.cloned.1.call-start = ((), (), s32[]{:S(2)}) async-start(), calls=%async_computation.3 | async-start | bytes 1310720 | tf_op jit(solution)/shard_map/all_gather | solution.py:54
  13.6 108.1 %all-gather.16.cloned.1.call-start = ((), (), s32[]{:S(2)}) async-start(), calls=%async_computation.5 | async-start | bytes 1310720 | tf_op jit(solution)/shard_map/all_gather | solution.py:63
  14.4 57.6 %copy-start.8 = (f32[256]{0:T(256)S(1)}, f32[256]{0:T(256)}, u32[]{:S(2)}) copy-start(f32[256]{0:T(256)} %param.24) | copy-start | bytes 3076
  14.4 57.6 %copy-start.9 = (f32[256]{0:T(256)S(1)}, f32[256]{0:T(256)}, u32[]{:S(2)}) copy-start(f32[256]{0:T(256)} %param.23) | copy-start | bytes 3076
  14.4 143.9 %reduce-scatter.3.cloned.1.call-start = ((), (), s32[]{:S(2)}) async-start(), calls=%async_computation.6 | async-start | bytes 2621440 | tf_op jit(solution)/shard_map/reduce_scatter | solution.py:83
  28.4 44.0 %copy-start.5 = (f32[4,128]{1,0:T(4,128)S(1)}, f32[4,128]{1,0:T(4,128)}, u32[]{:S(2)}) copy-start(f32[4,128]{1,0:T(4,128)} %param.26) | copy-start | bytes 6148
  66.1 55.6 %copy-start.12 = (f32[256]{0:T(256)S(1)}, f32[256]{0:T(256)}, u32[]{:S(2)}) copy-start(f32[256]{0:T(256)} %param.20) | copy-start | bytes 3076
  121.7 36.7 %copy-start.1 = (bf16[128,2048]{1,0:T(8,128)(2,1)S(1)}, bf16[128,2048]{1,0:T(8,128)(2,1)}, u32[]{:S(2)}) copy-start(bf16[128,2048]{1,0:T(8,128)(2,1)} %param.17) | copy-start | bytes 1572868
  121.7 38.0 %copy-start.4 = (f32[2048]{0:T(1024)S(1)}, f32[2048]{0:T(1024)}, u32[]{:S(2)}) copy-start(f32[2048]{0:T(1024)} %param.29) | copy-start | bytes 24580
  127.6 56.8 %all-gather.18.cloned.1.call-start = ((), (), s32[]{:S(2)}) async-start(), calls=%async_computation.7 | async-start | bytes 2621440 | tf_op jit(solution)/shard_map/all_gather | solution.py:93
  161.7 173.9 %all-gather.20.cloned.1.call-start = ((), (), s32[]{:S(2)}) async-start(), calls=%async_computation.8 | async-start | bytes 10485760 | tf_op jit(solution)/shard_map/all_gather | solution.py:42
  165.6 4.0 copy-start.7
  165.6 319.4 %copy-start.10 = (f32[2048]{0:T(1024)S(1)}, f32[2048]{0:T(1024)}, u32[]{:S(2)}) copy-start(f32[2048]{0:T(1024)} %param.31) | copy-start | bytes 24580
  165.6 319.4 %all-gather.22.cloned.1.call-start = ((), (), s32[]{:S(2)}) async-start(), calls=%async_computation.9 | async-start | bytes 10485760 | tf_op jit(solution)/shard_map/all_gather | solution.py:43
  169.6 361.6 %reduce-scatter.5.cloned.1.call-start = ((), (), s32[]{:S(2)}) async-start(), calls=%async_computation.10 | async-start | bytes 2621440 | tf_op jit(solution)/shard_map/reduce_scatter | solution.py:97
  485.0 46.1 %copy-start.2 = (bf16[128,2048]{1,0:T(8,128)(2,1)S(1)}, bf16[128,2048]{1,0:T(8,128)(2,1)}, u32[]{:S(2)}) copy-start(bf16[128,2048]{1,0:T(8,128)(2,1)} %reduce-scatter.3.cloned.1.call-done) | copy-start | bytes 1572868
Sparse Core Ops, SparseCore 0:
  8.9 30.7 all-gather.13
  41.3 21.9 all-gather.9
  64.9 27.9 all-gather.11
  94.3 27.3 all-gather.15
  127.7 30.5 reduce-scatter.2
  161.8 22.5 all-gather.17
  186.0 149.5 all-gather.19
  337.2 147.7 all-gather.21
  501.8 29.3 reduce-scatter.4
where the time goes:
time: 540 us
  waiting for transfers between devices  446 us (83%)
  blocking collectives  31.9 us (6%)
  matrix products  25.6 us (5%)
  other arithmetic  20.9 us (4%)
  between operations  13.4 us (2%)
    all_gather x1, waiting for transfers between devices, body(): lax.all_gather(expand_half, 'fs', axis=0, tiled=True)  151 us
    all_gather x1, waiting for transfers between devices, body(): lax.all_gather(reduce_half, 'fs', axis=1, tiled=True)  149 us
    reduce_scatter x1, waiting for transfers between devices, body(): lax.psum_scatter((jnp.dot(rows, full_merge, preferred_element_type=jnp.fl...  30.7 us
    reduce_scatter x1, waiting for transfers between devices, body(): lax.psum_scatter((jnp.dot(rows, full_reduce, preferred_element_type=jnp.f...  29.5 us
    all_gather x1, waiting for transfers between devices, body(): lax.all_gather(merge_half, 'fs', axis=1, tiled=True)  28.8 us
    all_gather x1, waiting for transfers between devices, body(): whole = lax.all_gather(normed, 'tp', axis=0, tiled=True)  23.5 us
    all_gather x1, waiting for transfers between devices, body(): lax.all_gather(direct_half, 'fs', axis=0, tiled=True)  19.1 us
    dot_general x1, matrix products, body(): jnp.dot(rows, full_reduce, preferred_element_type=jnp.float32)  16.6 us
  transfers between devices with their start and end apart: 9, of which 9 were waited for; matrix products, arithmetic and copies ran while one was open for 3% of the time, Pallas kernels for 0%

commit v1 on v0

--- a/solution.py
+++ b/solution.py
@@ -60,7 +60,7 @@
         preferred_element_type=jnp.float32,
     )
     full_merge, merge_full_scale = (
-        lax.all_gather(merge_half, "fs", axis=1, tiled=True),
+        jnp.concatenate(lax.all_gather(merge_half, "fs"), axis=1),
         lax.all_gather(merge_scale.astype(jnp.bfloat16), "fs", axis=0, tiled=True).astype(
             merge_scale.dtype
         ),

time: 540 us -> 540 us (level)
    all_gather x1, waiting for transfers between devices: 28.8 us -> 11.3 us  [body(): lax.all_gather(merge_half, 'fs')]
    all_gather x1, waiting for transfers between devices: 11.3 us -> 27.4 us  [body(): lax.all_gather(value_half, 'fs', axis=0, tiled=True)]
  transfers between devices with their start and end apart: 9 -> 9, of which waited for: 9 -> 9; matrix products, arithmetic and copies ran while one was open for 3% -> 4% of each run, Pallas kernels for 0% -> 0%
where the time goes in v1:
time: 540 us; the launch traced here: 539 us
  waiting for transfers between devices  445 us (82%)
  blocking collectives  31.9 us (6%)
  matrix products  25.2 us (5%)
  other arithmetic  20.9 us (4%)
  between operations  13.4 us (2%)
    all_gather x1, waiting for transfers between devices, body(): lax.all_gather(expand_half, 'fs', axis=0, tiled=True)  151 us
    all_gather x1, waiting for transfers between devices, body(): lax.all_gather(reduce_half, 'fs', axis=1, tiled=True)  149 us
    reduce_scatter x1, waiting for transfers between devices, body(): lax.psum_scatter((jnp.dot(rows, full_merge, preferred_element_type=jnp.fl...  30.7 us
    reduce_scatter x1, waiting for transfers between devices, body(): lax.psum_scatter((jnp.dot(rows, full_reduce, preferred_element_type=jnp.f...  29.5 us
    all_gather x1, waiting for transfers between devices, body(): lax.all_gather(value_half, 'fs', axis=0, tiled=True)  27.4 us
    all_gather x1, waiting for transfers between devices, body(): whole = lax.all_gather(normed, 'tp', axis=0, tiled=True)  23.5 us
    all_gather x1, waiting for transfers between devices, body(): lax.all_gather(direct_half, 'fs', axis=0, tiled=True)  18.9 us
    dot_general x1, matrix products, body(): jnp.dot(rows, full_reduce, preferred_element_type=jnp.float32)  16.6 us
  transfers between devices with their start and end apart: 9, of which 9 were waited for; matrix products, arithmetic and copies ran while one was open for 4% of the time, Pallas kernels for 0%

profile of v1, /device:TPU:0, one launch (start us, length us, event | category | flops | bytes accessed | tf_op | source)
XLA Modules:
  0.0 539.4 jit_solution(17999194710954520992)
XLA Ops:
  6.5 0.0 all-gather.23.cloned.1.call-start
  6.6 1.8 convert_element_type.74
  8.4 0.0 all-gather.23.cloned.1.call-update
  8.5 0.0 all-gather.15.cloned.1.call-start
  8.5 1.8 convert_element_type.71
  10.3 0.0 all-gather.15.cloned.1.call-update
  10.3 0.0 all-gather.11.cloned.1.call-start
  10.3 1.2 fusion.1
  11.6 2.0 fusion.3
  13.6 0.0 all-gather.11.cloned.1.call-update
  13.6 0.0 all-gather.13.cloned.1.call-start
  13.7 0.7 convert_element_type.70
  14.4 0.0 all-gather.13.cloned.1.call-update
  14.4 0.0 reduce-scatter.3.cloned.1.call-start
  14.5 13.9 %all-gather.1 = bf16[4,1,512]{2,1,0:T(2,128)(2,1)S(1)} all-gather(bf16[1,1,512]{2,1,0:T(2,128)(2,1)S(1)} %reshape.49), channel_id=1, replica_groups=mesh['rep'=2,'fs'=4,'tp'=4] {'fs'}, dimensions={0}, use_global_device_ids=true | all-gather | bytes 5120 | tf_op jit(solution)/shard_map/all_gather | solution.py:64
  28.4 11.3 %all-gather.23.cloned.1.call-done = bf16[1024,512]{1,0:T(8,128)(2,1)} async-done(((bf16[256,512]{1,0:T(8,128)(2,1)}), bf16[1024,512]{1,0:T(8,128)(2,1)}) %all-gather.23.cloned.1.call-update) | async-done | bytes 1048592 | tf_op jit(solution)/shard_map/all_gather | solution.py:63
  39.7 1.5 copy.37
  41.3 27.4 %all-gather.15.cloned.1.call-done = bf16[2048,256]{1,0:T(8,128)(2,1)} async-done(((bf16[512,256]{1,0:T(8,128)(2,1)}), bf16[2048,256]{1,0:T(8,128)(2,1)}) %all-gather.15.cloned.1.call-update) | async-done | bytes 1048592 | tf_op jit(solution)/shard_map/all_gather | solution.py:59
  68.7 23.5 %all-gather.11.cloned.1.call-done = bf16[512,2048]{1,0:T(8,128)(2,1)} async-done(((bf16[128,2048]{1,0:T(8,128)(2,1)}), bf16[512,2048]{1,0:T(8,128)(2,1)}) %all-gather.11.cloned.1.call-update) | async-done | bytes 2097168 | tf_op jit(solution)/shard_map/all_gather | solution.py:49
  92.2 2.8 fusion.37
  95.0 5.9 %all-reduce = (f32[512]{0:T(512)S(1)}, f32[512]{0:T(512)S(1)}) all-reduce(f32[512]{0:T(512)S(1)} %get-tuple-element.6, f32[512]{0:T(512)S(1)} %get-tuple-element.5), channel_id=1, replica_groups=mesh['rep'=2,'fs'=4,'tp'=4] {'tp'}, use_global_device_ids=true, to_apply=%region_4.0 | all-reduce | flops 1024 | bytes 8192 | tf_op jit(solution)/shard_map/psum | solution.py:70
  100.9 0.2 add_convert_fusion
  101.2 0.2 reshape.56
  101.4 0.3 fusion
  101.7 0.4 copy.42
  102.2 0.6 reshape.57
  102.8 18.9 %all-gather.13.cloned.1.call-done = bf16[2048,256]{1,0:T(8,128)(2,1)} async-done(((bf16[512,256]{1,0:T(8,128)(2,1)}), bf16[2048,256]{1,0:T(8,128)(2,1)}) %all-gather.13.cloned.1.call-update) | async-done | bytes 1048592 | tf_op jit(solution)/shard_map/all_gather | solution.py:54
  121.7 5.6 %multiply_convert_fusion.2 = bf16[512,2048]{1,0:T(8,128)(2,1)} fusion(bf16[256,2048]{0,1:T(8,128)(2,1)S(1)} %bitcast.25, f32[2048]{0:T(1024)S(1)} %bitcast.26, f32[512,256]{1,0:T(8,128)S(1)} %reshape.57, bf16[512,2048]{1,0:T(8,128)(2,1)} %all-gather.11.cloned.1.call-done, bf16[2048,256]{1,0:T(8,128)(2,1)} %all-gather.13.cloned.1.call-done, f32[256]{0:T(256)S(1)} %copy-done.12), kind=kOutput, calls=%fused_computation.2 | convolution fusion | flops 1077280768 | bytes 6824960 | tf_op jit(solution)/shard_map/dot_general | solution.py:84
  127.3 0.0 reduce-scatter.3.cloned.1.call-update
  127.3 0.0 all-gather.17.cloned.1.call-start
  127.4 30.7 %reduce-scatter.3.cloned.1.call-done = bf16[128,2048]{1,0:T(8,128)(2,1)} async-done(((bf16[512,2048]{1,0:T(8,128)(2,1)}), bf16[128,2048]{1,0:T(8,128)(2,1)}) %reduce-scatter.3.cloned.1.call-update) | async-done | bytes 524304 | tf_op jit(solution)/shard_map/reduce_scatter | solution.py:83
  158.0 1.3 fusion.5
  159.3 2.0 fusion.7
  161.4 0.0 all-gather.17.cloned.1.call-update
  161.4 0.0 all-gather.19.cloned.1.call-start
  161.5 3.8 convert_element_type.82
  165.3 0.0 all-gather.19.cloned.1.call-update
  165.3 0.0 all-gather.21.cloned.1.call-start
  165.4 3.9 convert_element_type.84
  169.2 0.0 reduce-scatter.5.cloned.1.call-start
  169.3 12.1 %all-gather.2 = bf16[4,1,512]{2,1,0:T(2,128)(2,1)S(1)} all-gather(bf16[1,1,512]{2,1,0:T(2,128)(2,1)S(1)} %reshape.51), channel_id=1, replica_groups=mesh['rep'=2,'fs'=4,'tp'=4] {'fs'}, dimensions={0}, use_global_device_ids=true | all-gather | bytes 5120 | tf_op jit(solution)/shard_map/all_gather | solution.py:44
  181.5 2.7 all-gather.17.cloned.1.call-done
  184.1 151.2 %all-gather.19.cloned.1.call-done = bf16[2048,2048]{1,0:T(8,128)(2,1)} async-done(((bf16[512,2048]{1,0:T(8,128)(2,1)}), bf16[2048,2048]{1,0:T(8,128)(2,1)}) %all-gather.19.cloned.1.call-update) | async-done | bytes 8388624 | tf_op jit(solution)/shard_map/all_gather | solution.py:42
  335.3 149.4 %all-gather.21.cloned.1.call-done = bf16[2048,2048]{1,0:T(8,128)(2,1)} async-done(((bf16[2048,512]{1,0:T(8,128)(2,1)}), bf16[2048,2048]{1,0:T(8,128)(2,1)}) %all-gather.21.cloned.1.call-update) | async-done | bytes 8388624 | tf_op jit(solution)/shard_map/all_gather | solution.py:43
  484.7 16.6 %multiply_convert_fusion = bf16[512,2048]{1,0:T(8,128)(2,1)} fusion(bf16[2048,2048]{1,0:T(8,128)(2,1)} %all-gather.21.cloned.1.call-done, f32[2048]{0:T(1024)S(1)} %bitcast.27, bf16[512,2048]{1,0:T(8,128)(2,1)} %all-gather.17.cloned.1.call-done, bf16[2048,2048]{1,0:T(8,128)(2,1)} %all-gather.19.cloned.1.call-done, f32[2048]{0:T(1024)S(1)} %copy-done.10), kind=kOutput, calls=%fused_computation | convolution fusion | flops 8596226048 | bytes 20987904 | tf_op jit(solution)/shard_map/dot_general | solution.py:98
  501.3 0.0 reduce-scatter.5.cloned.1.call-update
  501.3 29.5 %reduce-scatter.5.cloned.1.call-done = bf16[128,2048]{1,0:T(8,128)(2,1)} async-done(((bf16[512,2048]{1,0:T(8,128)(2,1)}), bf16[128,2048]{1,0:T(8,128)(2,1)}) %reduce-scatter.5.cloned.1.call-update) | async-done | bytes 524304 | tf_op jit(solution)/shard_map/reduce_scatter | solution.py:97
  530.8 2.1 fusion.8
  (36 shorter events, 0.1 us)
Async XLA Ops:
  6.5 94.9 %copy-start = (bf16[4,128,128]{2,1,0:T(8,128)(2,1)S(1)}, bf16[4,128,128]{2,1,0:T(8,128)(2,1)}, u32[]{:S(2)}) copy-start(bf16[4,128,128]{2,1,0:T(8,128)(2,1)} %param.25) | copy-start | bytes 393220
  6.5 7.2 %copy-start.3 = (f32[512,256]{1,0:T(8,128)S(1)}, f32[512,256]{1,0:T(8,128)}, u32[]{:S(2)}) copy-start(f32[512,256]{1,0:T(8,128)} %param.19) | copy-start | bytes 1572868
  6.5 8.0 %copy-start.6 = (f32[512]{0:T(512)S(1)}, f32[512]{0:T(512)}, u32[]{:S(2)}) copy-start(f32[512]{0:T(512)} %param.28) | copy-start | bytes 6148
  6.5 85.7 %copy-start.11 = (f32[256]{0:T(256)S(1)}, f32[256]{0:T(256)}, u32[]{:S(2)}) copy-start(f32[256]{0:T(256)} %param.22) | copy-start | bytes 3076
  6.5 33.2 %all-gather.23.cloned.1.call-start = ((), (), s32[]{:S(2)}) async-start(), calls=%async_computation.10 | async-start | bytes 1310720 | tf_op jit(solution)/shard_map/all_gather | solution.py:63
  8.5 60.2 %all-gather.15.cloned.1.call-start = ((), (), s32[]{:S(2)}) async-start(), calls=%async_computation.4 | async-start | bytes 1310720 | tf_op jit(solution)/shard_map/all_gather | solution.py:59
  10.3 81.9 %all-gather.11.cloned.1.call-start = ((), (), s32[]{:S(2)}) async-start(), calls=%async_computation.2 | async-start | bytes 2621440 | tf_op jit(solution)/shard_map/all_gather | solution.py:49
  13.6 108.0 %all-gather.13.cloned.1.call-start = ((), (), s32[]{:S(2)}) async-start(), calls=%async_computation.3 | async-start | bytes 1310720 | tf_op jit(solution)/shard_map/all_gather | solution.py:54
  14.4 143.6 %reduce-scatter.3.cloned.1.call-start = ((), (), s32[]{:S(2)}) async-start(), calls=%async_computation.5 | async-start | bytes 2621440 | tf_op jit(solution)/shard_map/reduce_scatter | solution.py:83
  41.2 59.7 %copy-start.8 = (f32[256]{0:T(256)S(1)}, f32[256]{0:T(256)}, u32[]{:S(2)}) copy-start(f32[256]{0:T(256)} %param.24) | copy-start | bytes 3076
  41.2 59.7 %copy-start.9 = (f32[256]{0:T(256)S(1)}, f32[256]{0:T(256)}, u32[]{:S(2)}) copy-start(f32[256]{0:T(256)} %param.23) | copy-start | bytes 3076
  41.2 60.2 %copy-start.5 = (f32[4,128]{1,0:T(4,128)S(1)}, f32[4,128]{1,0:T(4,128)}, u32[]{:S(2)}) copy-start(f32[4,128]{1,0:T(4,128)} %param.26) | copy-start | bytes 6148
  95.0 26.7 %copy-start.12 = (f32[256]{0:T(256)S(1)}, f32[256]{0:T(256)}, u32[]{:S(2)}) copy-start(f32[256]{0:T(256)} %param.20) | copy-start | bytes 3076
  121.7 36.3 %copy-start.1 = (bf16[128,2048]{1,0:T(8,128)(2,1)S(1)}, bf16[128,2048]{1,0:T(8,128)(2,1)}, u32[]{:S(2)}) copy-start(bf16[128,2048]{1,0:T(8,128)(2,1)} %param.17) | copy-start | bytes 1572868
  121.7 37.6 %copy-start.4 = (f32[2048]{0:T(1024)S(1)}, f32[2048]{0:T(1024)}, u32[]{:S(2)}) copy-start(f32[2048]{0:T(1024)} %param.29) | copy-start | bytes 24580
  127.3 56.8 %all-gather.17.cloned.1.call-start = ((), (), s32[]{:S(2)}) async-start(), calls=%async_computation.6 | async-start | bytes 2621440 | tf_op jit(solution)/shard_map/all_gather | solution.py:93
  161.4 173.9 %all-gather.19.cloned.1.call-start = ((), (), s32[]{:S(2)}) async-start(), calls=%async_computation.7 | async-start | bytes 10485760 | tf_op jit(solution)/shard_map/all_gather | solution.py:42
  165.3 4.0 copy-start.7
  165.3 319.4 %copy-start.10 = (f32[2048]{0:T(1024)S(1)}, f32[2048]{0:T(1024)}, u32[]{:S(2)}) copy-start(f32[2048]{0:T(1024)} %param.31) | copy-start | bytes 24580
  165.3 319.4 %all-gather.21.cloned.1.call-start = ((), (), s32[]{:S(2)}) async-start(), calls=%async_computation.8 | async-start | bytes 10485760 | tf_op jit(solution)/shard_map/all_gather | solution.py:43
  169.2 361.6 %reduce-scatter.5.cloned.1.call-start = ((), (), s32[]{:S(2)}) async-start(), calls=%async_computation.9 | async-start | bytes 2621440 | tf_op jit(solution)/shard_map/reduce_scatter | solution.py:97
  484.7 46.1 %copy-start.2 = (bf16[128,2048]{1,0:T(8,128)(2,1)S(1)}, bf16[128,2048]{1,0:T(8,128)(2,1)}, u32[]{:S(2)}) copy-start(bf16[128,2048]{1,0:T(8,128)(2,1)} %reduce-scatter.3.cloned.1.call-done) | copy-start | bytes 1572868
Sparse Core Ops, SparseCore 0:
  8.9 30.7 all-gather.22
  41.3 27.3 all-gather.14
  70.3 21.9 all-gather.10
  93.7 27.9 all-gather.12
  127.4 30.5 reduce-scatter.2
  161.5 22.5 all-gather.16
  185.7 149.5 all-gather.18
  336.9 147.7 all-gather.20
  501.4 29.3 reduce-scatter.4
